TPU v7x, 32 devices: a whole 2x2x4 slice. The times are simulated.
32 devices in a mesh: rep: 4 (over z), fs: 4 (over y, x), tp: 2 (over core).
Axes of the slice: x: 2, y: 2, z: 4, core: 2. Of those that a mesh axis runs over, the one named last changes fastest.
Arguments:
- hidden_in: bfloat16 [2048, 2048], P('rep'), may hold values from -6 to 6
- cotangent: bfloat16 [2048, 2048], P('rep'), may hold values from -3 to 3
- w_up: bfloat16 [2048, 8192], P('rep', ('fs', 'tp')), may hold values from -0.125 to 0.125
- w_down: bfloat16 [8192, 2048], P(('fs', 'tp'), 'rep'), may hold values from -0.0625 to 0.0625
Outputs:
- input_grad: bfloat16 [2048, 2048], P('rep')
- up_grad: float32 [2048, 8192], P('rep', ('fs', 'tp'))
- down_grad: float32 [8192, 2048], P(('fs', 'tp'), 'rep')
All inputs are finite; a program needn't handle non-finite values.
Results may differ from a plain program's by a relative error of at most 0.017.
Values may be sent and summed in bfloat16 or wider, within the bound.
A program may use at most 64 MiB of HBM per device.

v0:
```python
import jax
import jax.numpy as jnp
from jax import lax
from jax.sharding import PartitionSpec as P


def contract_last(left, right):
    return lax.dot_general(
        left, right, (((1,), (1,)), ((), ())), preferred_element_type=jnp.float32
    )


def contract_first(left, right):
    return lax.dot_general(
        left, right, (((0,), (0,)), ((), ())), preferred_element_type=jnp.float32
    )


def on_device(hidden_in, cotangent, w_up, w_down):
    up_full = lax.all_gather(w_up, "rep", axis=0, tiled=True)
    back_grad = contract_last(cotangent, lax.all_gather(w_down, "rep", axis=1, tiled=True))
    preact = jnp.dot(hidden_in, up_full, preferred_element_type=jnp.float32)
    active = jnp.maximum(preact, 0.0)
    hidden = (active * active).astype(jnp.bfloat16)
    slopes = (2.0 * active * back_grad).astype(jnp.bfloat16)
    grad_upper = lax.psum_scatter(
        contract_first(hidden_in, slopes).astype(jnp.bfloat16),
        "rep",
        scatter_dimension=0,
        tiled=True,
    ).astype(jnp.float32)
    lower_rows = lax.psum_scatter(
        contract_first(cotangent, hidden).astype(jnp.bfloat16),
        "rep",
        scatter_dimension=0,
        tiled=True,
    ).astype(jnp.float32)
    down_grad = lower_rows.T
    partial_sum = contract_last(slopes, up_full).astype(jnp.bfloat16)
    input_grad = lax.psum(partial_sum, ("fs", "tp")).astype(jnp.float32).astype(jnp.bfloat16)
    return (input_grad, grad_upper, down_grad)


def solution(mesh):
    return jax.shard_map(
        on_device,
        mesh=mesh,
        in_specs=(P("rep", None), P("rep", None), P("rep", ("fs", "tp")), P(("fs", "tp"), "rep")),
        out_specs=(P("rep", None), P("rep", ("fs", "tp")), P(("fs", "tp"), "rep")),
        check_vma=False,
    )
```

profile of v0, /device:TPU:0, one launch (start us, length us, event | category | flops | bytes accessed | tf_op | source)
XLA Modules:
  0.0 414.7 jit_solution(14841434194789787365)
XLA Ops:
  7.2 0.0 copy-start
  7.2 0.0 all-gather.3.cloned.1.call-start
  7.2 0.7 all-gather.3.cloned.1.call-update
  7.9 0.0 all-gather.5.cloned.1.call-start
  8.0 0.7 all-gather.5.cloned.1.call-update
  8.7 0.0 reduce-scatter.3.cloned.1.call-start
  8.7 84.3 %all-gather.3.cloned.1.call-done = bf16[2048,1024]{1,0:T(8,128)(2,1)} async-done(((bf16[512,1024]{1,0:T(8,128)(2,1)}), bf16[2048,1024]{1,0:T(8,128)(2,1)}) %all-gather.3.cloned.1.call-update) | async-done | bytes 4194320 | tf_op jit(solution)/shard_map/all_gather | solution.py:20
  93.1 5.8 %fusion.2 = f32[512,1024]{1,0:T(8,128)} fusion(bf16[512,2048]{1,0:T(8,128)(2,1)S(1)} %copy-done, bf16[2048,1024]{1,0:T(8,128)(2,1)} %all-gather.3.cloned.1.call-done), kind=kOutput, calls=%fused_computation.8 | convolution fusion | flops 2147483648 | bytes 8388608 | tf_op jit(solution)/shard_map/dot_general | solution.py:22
  98.9 75.0 %all-gather.5.cloned.1.call-done = bf16[1024,2048]{1,0:T(8,128)(2,1)} async-done(((bf16[1024,512]{1,0:T(8,128)(2,1)}), bf16[1024,2048]{1,0:T(8,128)(2,1)}) %all-gather.5.cloned.1.call-update) | async-done | bytes 4194320 | tf_op jit(solution)/shard_map/all_gather | solution.py:21
  173.9 5.8 %multiply_convert_fusion.1 = bf16[512,1024]{1,0:T(8,128)(2,1)S(1)} fusion(f32[512,1024]{1,0:T(8,128)} %fusion.2, bf16[512,2048]{1,0:T(8,128)(2,1)} %param.5, bf16[1024,2048]{1,0:T(8,128)(2,1)} %all-gather.5.cloned.1.call-done), kind=kOutput, calls=%fused_computation.5 | convolution fusion | flops 2149580800 | bytes 9437184 | tf_op jit(solution)/shard_map/dot_general | solution.py:8
  179.7 4.4 %convert_bitcast_fusion.1 = bf16[2048,1024]{0,1:T(8,128)(2,1)} fusion(bf16[512,1024]{1,0:T(8,128)(2,1)S(1)} %multiply_convert_fusion.1, bf16[512,2048]{1,0:T(8,128)(2,1)S(1)} %copy-done), kind=kOutput, calls=%fused_computation.1 | convolution fusion | flops 2149580800 | bytes 7340032 | tf_op jit(solution)/shard_map/dot_general | solution.py:14
  184.1 0.0 reduce-scatter.3.cloned.1.call-update
  184.1 0.0 reduce-scatter.5.cloned.1.call-start
  184.2 6.6 %convert_bitcast_fusion = bf16[2048,1024]{0,1:T(8,128)(2,1)} fusion(bf16[512,2048]{1,0:T(8,128)(2,1)} %param.5, f32[512,1024]{1,0:T(8,128)} %fusion.2), kind=kOutput, calls=%fused_computation | convolution fusion | flops 2151153664 | bytes 8388608 | tf_op jit(solution)/shard_map/dot_general | solution.py:14
  190.8 0.0 reduce-scatter.5.cloned.1.call-update
  190.8 0.0 all-reduce.2.cloned.1.call-start
  190.8 5.9 %convolution_convert_fusion = bf16[512,2048]{1,0:T(8,128)(2,1)} fusion(bf16[512,1024]{1,0:T(8,128)(2,1)S(1)} %multiply_convert_fusion.1, bf16[2048,1024]{1,0:T(8,128)(2,1)} %all-gather.3.cloned.1.call-done), kind=kOutput, calls=%fused_computation.2 | convolution fusion | flops 2148532224 | bytes 7340032 | tf_op jit(solution)/shard_map/dot_general | solution.py:8
  196.7 0.0 all-reduce.2.cloned.1.call-update
  196.7 62.8 %reduce-scatter.3.cloned.1.call-done = bf16[512,1024]{0,1:T(8,128)(2,1)} async-done(((bf16[2048,1024]{0,1:T(8,128)(2,1)}), bf16[512,1024]{0,1:T(8,128)(2,1)}) %reduce-scatter.3.cloned.1.call-update) | async-done | bytes 1048592 | tf_op jit(solution)/shard_map/reduce_scatter | solution.py:26
  259.6 2.6 copy.7
  262.1 76.9 %reduce-scatter.5.cloned.1.call-done = bf16[512,1024]{0,1:T(8,128)(2,1)} async-done(((bf16[2048,1024]{0,1:T(8,128)(2,1)}), bf16[512,1024]{0,1:T(8,128)(2,1)}) %reduce-scatter.5.cloned.1.call-update) | async-done | bytes 1048592 | tf_op jit(solution)/shard_map/reduce_scatter | solution.py:32
  339.1 2.8 convert_bitcast_fusion.2
  341.9 63.1 %all-reduce.2.cloned.1.call-done = bf16[512,2048]{1,0:T(8,128)(2,1)} async-done(((bf16[512,2048]{1,0:T(8,128)(2,1)}), bf16[512,2048]{1,0:T(8,128)(2,1)}) %all-reduce.2.cloned.1.call-update) | async-done | bytes 2097168 | tf_op jit(solution)/shard_map/psum | solution.py:40
  405.0 3.2 copy.9
  (1 shorter events, 0.0 us)
Async XLA Ops:
  7.2 85.9 %copy-start = (bf16[512,2048]{1,0:T(8,128)(2,1)S(1)}, bf16[512,2048]{1,0:T(8,128)(2,1)}, u32[]{:S(2)}) copy-start(bf16[512,2048]{1,0:T(8,128)(2,1)} %param.4) | copy-start | bytes 6291460
  7.2 85.9 %all-gather.3.cloned.1.call-start = ((), (), s32[]{:S(2)}) async-start(), calls=%async_computation.2 | async-start | bytes 5242880 | tf_op jit(solution)/shard_map/all_gather | solution.py:20
  7.9 166.0 %all-gather.5.cloned.1.call-start = ((), (), s32[]{:S(2)}) async-start(), calls=%async_computation.3 | async-start | bytes 5242880 | tf_op jit(solution)/shard_map/all_gather | solution.py:21
  8.7 250.9 %reduce-scatter.3.cloned.1.call-start = ((), (), s32[]{:S(2)}) async-start(), calls=%async_computation.5 | async-start | bytes 5242880 | tf_op jit(solution)/shard_map/reduce_scatter | solution.py:26
  184.1 154.9 %reduce-scatter.5.cloned.1.call-start = ((), (), s32[]{:S(2)}) async-start(), calls=%async_computation.6 | async-start | bytes 5242880 | tf_op jit(solution)/shard_map/reduce_scatter | solution.py:32
  190.8 214.2 %all-reduce.2.cloned.1.call-start = ((), (), s32[]{:S(2)}) async-start(), calls=%async_computation.4 | async-start | bytes 4194304 | tf_op jit(solution)/shard_map/psum | solution.py:40
Sparse Core Ops, SparseCore 0:
  9.6 83.4 all-gather.2
  94.6 79.2 all-gather.4
  184.3 75.2 reduce-scatter.2
  261.7 77.2 reduce-scatter.4
  342.7 62.2 all-reduce.1
where the time goes:
time: 415 us
  waiting for transfers between devices  364 us (88%)
  matrix products  28.5 us (7%)
  between operations  13.8 us (3%)
  local copies, waits for them, and re-layouts  5.73 us (1%)
    all_gather x1, waiting for transfers between devices, on_device(): up_full = lax.all_gather(w_up, 'rep', axis=0, tiled=True)  84.3 us
    reduce_scatter x1, waiting for transfers between devices, on_device(): lax.psum_scatter(contract_first(cotangent, hidden).astype(jnp.bfloat16),...  76.9 us
    all_gather x1, waiting for transfers between devices, on_device(): lax.all_gather(w_down, 'rep', axis=1, tiled=True)  75 us
    psum x1, waiting for transfers between devices, on_device(): lax.psum(partial_sum, ('fs', 'tp')).astype(jnp.float32).astype(jnp.bfloat16)  63.1 us
    reduce_scatter x1, waiting for transfers between devices, on_device(): lax.psum_scatter(contract_first(hidden_in, slopes).astype(jnp.bfloat16),...  62.8 us
    dot_general x2, matrix products, contract_last(): lax.dot_general(left, right, (((1,), (1,)), ((), ())), preferred_element_...  11.7 us
    dot_general x2, matrix products, contract_first(): lax.dot_general(left, right, (((0,), (0,)), ((), ())), preferred_element_...  10.9 us
  transfers between devices with their start and end apart: 5, of which 5 were waited for; matrix products, arithmetic and copies ran while one was open for 6% of the time, Pallas kernels for 0%

commit v1 on v0

--- a/solution.py
+++ b/solution.py
@@ -1,7 +1,16 @@
+import functools
 import jax
 import jax.numpy as jnp
 from jax import lax
 from jax.sharding import PartitionSpec as P
+
+
+def start_signs(inputs, peer_axis, axis_key):
+    w2 = lax.psum(inputs, peer_axis)
+    return lax.psum(w2, axis_key)
+
+
+part_ends = functools.partial(start_signs, peer_axis="tp", axis_key="fs")
 
 
 def contract_last(left, right):
@@ -37,7 +46,7 @@
     ).astype(jnp.float32)
     down_grad = lower_rows.T
     partial_sum = contract_last(slopes, up_full).astype(jnp.bfloat16)
-    input_grad = lax.psum(partial_sum, ("fs", "tp")).astype(jnp.float32).astype(jnp.bfloat16)
+    input_grad = part_ends(partial_sum).astype(jnp.float32).astype(jnp.bfloat16)
     return (input_grad, grad_upper, down_grad)
 
 

time: 415 us -> 446 us (1.075)
  waiting for transfers between devices: 364 us -> 397 us
    reduce_scatter x1, waiting for transfers between devices: 62.8 us -> 80.1 us  [on_device(): lax.psum_scatter(contract_first(hidden_in, slopes).astype(jnp.bfloat16),...]
    psum x1 -> x2, waiting for transfers between devices: 63.1 us -> 78.9 us  [the longest x1 70.1 us: start_signs(): return lax.psum(w2, axis_key)]
  transfers between devices with their start and end apart: 5 -> 6, of which waited for: 5 -> 6; matrix products, arithmetic and copies ran while one was open for 6% -> 5% of each run, Pallas kernels for 0% -> 0%
where the time goes in v1:
time: 446 us
  waiting for transfers between devices  397 us (89%)
  matrix products  26.5 us (6%)
  between operations  14.1 us (3%)
  local copies, waits for them, and re-layouts  5.73 us (1%)
    all_gather x1, waiting for transfers between devices, on_device(): up_full = lax.all_gather(w_up, 'rep', axis=0, tiled=True)  84.3 us
    reduce_scatter x1, waiting for transfers between devices, on_device(): lax.psum_scatter(contract_first(hidden_in, slopes).astype(jnp.bfloat16),...  80.1 us
    reduce_scatter x1, waiting for transfers between devices, on_device(): lax.psum_scatter(contract_first(cotangent, hidden).astype(jnp.bfloat16),...  76.9 us
    all_gather x1, waiting for transfers between devices, on_device(): lax.all_gather(w_down, 'rep', axis=1, tiled=True)  75 us
    psum x1, waiting for transfers between devices, start_signs(): return lax.psum(w2, axis_key)  70.1 us
    dot_general x2, matrix products, contract_first(): lax.dot_general(left, right, (((0,), (0,)), ((), ())), preferred_element_...  11 us
    dot_general x2, matrix products, contract_last(): lax.dot_general(left, right, (((1,), (1,)), ((), ())), preferred_element_...  9.71 us
  transfers between devices with their start and end apart: 6, of which 6 were waited for; matrix products, arithmetic and copies ran while one was open for 5% of the time, Pallas kernels for 0%

profile of v1, /device:TPU:0, one launch (start us, length us, event | category | flops | bytes accessed | tf_op | source)
XLA Modules:
  0.0 446.2 jit_solution(2885865988723922395)
XLA Ops:
  7.2 0.0 all-gather.3.cloned.1.call-start
  7.2 0.7 all-gather.3.cloned.1.call-update
  7.9 0.0 all-gather.5.cloned.1.call-start
  8.0 0.7 all-gather.5.cloned.1.call-update
  8.7 0.0 all-reduce.3.cloned.1.call-start
  8.7 84.3 %all-gather.3.cloned.1.call-done = bf16[2048,1024]{1,0:T(8,128)(2,1)} async-done(((bf16[512,1024]{1,0:T(8,128)(2,1)}), bf16[2048,1024]{1,0:T(8,128)(2,1)}) %all-gather.3.cloned.1.call-update) | async-done | bytes 4194320 | tf_op jit(solution)/shard_map/all_gather | solution.py:29
  93.1 5.8 %fusion.2 = f32[512,1024]{1,0:T(8,128)} fusion(bf16[512,2048]{1,0:T(8,128)(2,1)S(1)} %copy-done, bf16[2048,1024]{1,0:T(8,128)(2,1)} %all-gather.3.cloned.1.call-done), kind=kOutput, calls=%fused_computation.8 | convolution fusion | flops 2147483648 | bytes 8388608 | tf_op jit(solution)/shard_map/dot_general | solution.py:31
  98.9 75.0 %all-gather.5.cloned.1.call-done = bf16[1024,2048]{1,0:T(8,128)(2,1)} async-done(((bf16[1024,512]{1,0:T(8,128)(2,1)}), bf16[1024,2048]{1,0:T(8,128)(2,1)}) %all-gather.5.cloned.1.call-update) | async-done | bytes 4194320 | tf_op jit(solution)/shard_map/all_gather | solution.py:30
  173.9 6.0 %multiply_convert_fusion.1 = bf16[512,1024]{1,0:T(8,128)(2,1)S(1)} fusion(f32[512,1024]{1,0:T(8,128)} %fusion.2, bf16[512,2048]{1,0:T(8,128)(2,1)} %param.5, bf16[1024,2048]{1,0:T(8,128)(2,1)} %all-gather.5.cloned.1.call-done), kind=kOutput, calls=%fused_computation.5 | convolution fusion | flops 2149580800 | bytes 9437184 | tf_op jit(solution)/shard_map/dot_general | solution.py:17
  179.9 3.7 convolution_convert_fusion
  183.6 0.0 all-reduce.3.cloned.1.call-update
  183.6 0.0 reduce-scatter.3.cloned.1.call-start
  183.7 4.3 convert_bitcast_fusion.1
  188.0 0.0 reduce-scatter.3.cloned.1.call-update
  188.0 0.0 reduce-scatter.5.cloned.1.call-start
  188.1 6.7 %convert_bitcast_fusion = bf16[2048,1024]{0,1:T(8,128)(2,1)} fusion(bf16[512,2048]{1,0:T(8,128)(2,1)} %param.5, f32[512,1024]{1,0:T(8,128)} %fusion.2), kind=kOutput, calls=%fused_computation | convolution fusion | flops 2151153664 | bytes 8388608 | tf_op jit(solution)/shard_map/dot_general | solution.py:23
  194.8 0.0 all-reduce.5.cloned.1.call-start
  194.8 8.7 %all-reduce.3.cloned.1.call-done = bf16[512,2048]{1,0:T(8,128)(2,1)} async-done(((bf16[512,2048]{1,0:T(8,128)(2,1)}), bf16[512,2048]{1,0:T(8,128)(2,1)}) %all-reduce.3.cloned.1.call-update) | async-done | bytes 2097168 | tf_op jit(solution)/shard_map/psum | solution.py:9
  203.6 80.1 %reduce-scatter.3.cloned.1.call-done = bf16[512,1024]{0,1:T(8,128)(2,1)} async-done(((bf16[2048,1024]{0,1:T(8,128)(2,1)}), bf16[512,1024]{0,1:T(8,128)(2,1)}) %reduce-scatter.3.cloned.1.call-update) | async-done | bytes 1048592 | tf_op jit(solution)/shard_map/reduce_scatter | solution.py:35
  283.7 2.6 copy.7
  286.3 76.9 %reduce-scatter.5.cloned.1.call-done = bf16[512,1024]{0,1:T(8,128)(2,1)} async-done(((bf16[2048,1024]{0,1:T(8,128)(2,1)}), bf16[512,1024]{0,1:T(8,128)(2,1)}) %reduce-scatter.5.cloned.1.call-update) | async-done | bytes 1048592 | tf_op jit(solution)/shard_map/reduce_scatter | solution.py:41
  363.2 2.8 convert_bitcast_fusion.2
  366.0 70.1 %all-reduce.5.cloned.1.call-done = bf16[512,2048]{1,0:T(8,128)(2,1)} async-done(((bf16[512,2048]{1,0:T(8,128)(2,1)}), bf16[512,2048]{1,0:T(8,128)(2,1)}) %all-reduce.5.cloned.1.call-update) | async-done | bytes 2097168 | tf_op jit(solution)/shard_map/psum | solution.py:10
  436.2 3.2 copy.10
  (6 shorter events, 0.0 us)
Async XLA Ops:
  7.2 85.9 %copy-start = (bf16[512,2048]{1,0:T(8,128)(2,1)S(1)}, bf16[512,2048]{1,0:T(8,128)(2,1)}, u32[]{:S(2)}) copy-start(bf16[512,2048]{1,0:T(8,128)(2,1)} %param.4) | copy-start | bytes 6291460
  7.2 85.9 %all-gather.3.cloned.1.call-start = ((), (), s32[]{:S(2)}) async-start(), calls=%async_computation.2 | async-start | bytes 5242880 | tf_op jit(solution)/shard_map/all_gather | solution.py:29
  7.9 166.0 %all-gather.5.cloned.1.call-start = ((), (), s32[]{:S(2)}) async-start(), calls=%async_computation.3 | async-start | bytes 5242880 | tf_op jit(solution)/shard_map/all_gather | solution.py:30
  8.7 194.9 %all-reduce.3.cloned.1.call-start = ((), (), s32[]{:S(2)}) async-start(), calls=%async_computation.4 | async-start | bytes 4194304 | tf_op jit(solution)/shard_map/psum | solution.py:9
  173.9 6.0 %copy-start.1 = (bf16[2048,1024]{1,0:T(8,128)(2,1)S(1)}, bf16[2048,1024]{1,0:T(8,128)(2,1)}, u32[]{:S(2)}) copy-start(bf16[2048,1024]{1,0:T(8,128)(2,1)} %all-gather.3.cloned.1.call-done) | copy-start | bytes 12582916
  183.6 100.1 %reduce-scatter.3.cloned.1.call-start = ((), (), s32[]{:S(2)}) async-start(), calls=%async_computation.6 | async-start | bytes 5242880 | tf_op jit(solution)/shard_map/reduce_scatter | solution.py:35
  188.0 175.2 %reduce-scatter.5.cloned.1.call-start = ((), (), s32[]{:S(2)}) async-start(), calls=%async_computation.7 | async-start | bytes 5242880 | tf_op jit(solution)/shard_map/reduce_scatter | solution.py:41
  194.8 241.4 %all-reduce.5.cloned.1.call-start = ((), (), s32[]{:S(2)}) async-start(), calls=%async_computation.5 | async-start | bytes 4194304 | tf_op jit(solution)/shard_map/psum | solution.py:10
Sparse Core Ops, SparseCore 0:
  9.6 83.4 all-gather.2
  94.6 79.2 all-gather.4
  183.8 19.7 all-reduce.2
  205.7 77.9 reduce-scatter.2
  285.8 77.2 reduce-scatter.4
  366.1 69.9 all-reduce.4
